TPU v7x, 32 devices: a whole 2x2x4 slice. The times are simulated.
32 devices in a mesh: ep: 4 (over y, x), tp: 8 (over z, core).
Axes of the slice: x: 2, y: 2, z: 4, core: 2. Of those that a mesh axis runs over, the one named last changes fastest.
Arguments:
- query_heads_rows: bfloat16 [2048, 2048], P('ep', 'tp'), may hold values from -9 to 9
- key_heads_rows: bfloat16 [2048, 2048], P('ep', 'tp'), may hold values from -9 to 9
- value_heads_rows: bfloat16 [2048, 2048], P('ep', 'tp'), may hold values from -6 to 6
- write_strength_logit: bfloat16 [16, 2048], P('tp', 'ep'), may hold values from -3.5 to -1
- decay_preactivation: bfloat16 [16, 2048], P('tp', 'ep'), may hold values from -5 to 5
- head_decay_logarithm: float32 [16], P('tp'), may hold values from -20 to -3
- extra_log_decay: float32 [16, 2048], P('tp', 'ep'), may hold values from -0.7 to 0
- output_weight: bfloat16 [2048, 2048], P('tp'), may hold values from -2 to 2
- second_batch_tokens: bfloat16 [4096, 2048], P(('ep', 'tp')), may hold values from -6 to 6
- expert_norm_scale: float32 [2048], replicated, may hold values from 0.1 to 1.9
- expert_choice_index: int32 [4096, 2], P(('ep', 'tp')), may hold values from 0 to 15, as said below
- group_router_weight: float32 [4096], P(('ep', 'tp')), may hold values from 0.25 to 1
- expert_logit_difference: float32 [4096], P(('ep', 'tp')), may hold values from -8 to 8
- expert_gate_weight: bfloat16 [16, 1024, 2048], P('ep', 'tp'), may hold values from -0.125 to 0.125
- expert_up_weight: bfloat16 [16, 1024, 2048], P('ep', 'tp'), may hold values from -0.125 to 0.125
- expert_down_weight: bfloat16 [16, 1024, 2048], P('ep', 'tp'), may hold values from -0.375 to 0.375
Outputs:
- mixer_output_first: bfloat16 [2048, 2048], P(('ep', 'tp'))
- expert_out: bfloat16 [4096, 2048], P(('ep', 'tp'))
Inputs may be any that keep to these rules, and one draw needn't show every extreme that they name: `expert_choice_index`: each row names two different experts of one group, the experts a * 4 to a * 4 + 3 for some a. In the rows of one device (aligned blocks of 128 rows) no expert is named more than 32 times, and in every device's rows some expert is named exactly 32 times.
All inputs are finite; a program needn't handle non-finite values.
Results may differ from a plain program's by a relative error of at most 0.018.
Values may be sent and summed in bfloat16 or wider, within the bound.
A program may use at most 128 MiB of HBM per device.

v0:
```python
import jax
import jax.numpy as jnp
from jax import lax
from jax.sharding import PartitionSpec as P

DK = 128
DV = 128
BLOCK = 64
CAP = 32
EXPERTS = 16
TOPK = 2
precise_setting = lax.Precision.HIGHEST
norm_eps = 1e-06


def prefix(value, axis, join, neutral):
    count, mine = (lax.axis_size(axis), lax.axis_index(axis))
    pieces = jax.tree.map(lambda part: lax.all_gather(part, axis), value)
    subtotal = jax.tree.map(
        lambda part, zero: jnp.full_like(part, 0) + jnp.asarray(zero, part.dtype), value, neutral
    )

    def step(position, subtotal):
        longer = join(subtotal, jax.tree.map(lambda part: part[position], pieces))
        return jax.tree.map(lambda new, old: jnp.where(position < mine, new, old), longer, subtotal)

    return lax.fori_loop(0, count - 1, step, subtotal)


def unit_rows(matrix):
    return matrix * lax.rsqrt(jnp.sum(matrix * matrix, axis=-1, keepdims=True) + norm_eps)


def block_terms(query_block, key_block, value_block, decay_logarithm, strength):
    span_len = query_block.shape[2]
    dim_value = value_block.shape[-1]
    cumulative = jnp.cumsum(decay_logarithm, axis=-1)
    within = jnp.tril(jnp.ones((span_len, span_len), bool))
    strict = jnp.tril(jnp.ones((span_len, span_len), bool), -1)
    spread = cumulative[..., :, None] - cumulative[..., None, :]
    decayed = jnp.where(within, jnp.exp(jnp.where(within, spread, 0.0)), 0.0)
    weighted = key_block * strength[..., None]
    lower_part = jnp.where(
        strict,
        jnp.einsum("hnid,hnjd->hnij", weighted, key_block, precision=precise_setting) * decayed,
        0.0,
    )
    system = lower_part + jnp.eye(span_len, dtype=jnp.float32)
    rhs_cols = jnp.concatenate(
        [value_block * strength[..., None], weighted * jnp.exp(cumulative)[..., None]], axis=-1
    )
    solved = jax.scipy.linalg.solve_triangular(system, rhs_cols, lower=True, unit_diagonal=True)
    updated_values = solved[..., :dim_value]
    delta_corrections = solved[..., dim_value:]
    scores = jnp.where(
        within,
        jnp.einsum("hnid,hnjd->hnij", query_block, key_block, precision=precise_setting) * decayed,
        0.0,
    )
    decayed_queries = query_block * jnp.exp(cumulative)[..., None]
    decayed_keys = key_block * jnp.exp(cumulative[..., -1:] - cumulative)[..., None]
    block_retention = jnp.exp(cumulative[..., -1])
    return (
        decayed_queries,
        decayed_keys,
        updated_values,
        delta_corrections,
        scores,
        block_retention,
    )


def carry_step(recurrent_state, inputs):
    decayed_queries, decayed_keys, updated_values, delta_corrections, scores, block_retention = (
        inputs
    )
    value_updates = updated_values - jnp.einsum(
        "jdb,jbu->jdu", delta_corrections, recurrent_state, precision=precise_setting
    )
    final_output = jnp.einsum(
        "jdb,jbu->jdu", decayed_queries, recurrent_state, precision=precise_setting
    )
    final_output = final_output + jnp.einsum(
        "hcj,hjv->hcv", scores, value_updates, precision=precise_setting
    )
    recurrent_state = recurrent_state * block_retention[:, None, None] + jnp.einsum(
        "rpq,rpd->rqd", decayed_keys, value_updates, precision=precise_setting
    )
    return (recurrent_state, final_output)


def compose(earlier, latter):
    joined_map = jnp.einsum("hij,hjk->hik", latter[0], earlier[0], precision=precise_setting)
    joined_state = (
        jnp.einsum("hij,hjv->hiv", latter[0], earlier[1], precision=precise_setting) + latter[1]
    )
    return (joined_map, joined_state)


def shards(
    query_heads_rows,
    key_heads_rows,
    value_heads_rows,
    write_strength_logit,
    decay_preactivation,
    head_decay_logarithm,
    extra_log_decay,
    output_weight,
    second_batch_tokens,
    expert_norm_scale,
    expert_choice_index,
    group_router_weight,
    expert_logit_difference,
    expert_gate_weight,
    expert_up_weight,
    expert_down_weight,
):
    length = query_heads_rows.shape[0]
    local_heads = head_decay_logarithm.shape[0]
    blocks = length // BLOCK
    width_model = output_weight.shape[1]

    def heads_first(matrix):
        spread_out = matrix.astype(jnp.float32).reshape(length, local_heads, -1).transpose(1, 0, 2)
        return spread_out.reshape(local_heads, blocks, BLOCK, -1)

    query_block = unit_rows(heads_first(query_heads_rows)) * DK ** (-0.5)
    key_block = unit_rows(heads_first(key_heads_rows))
    value_block = heads_first(value_heads_rows)
    strength = jax.nn.sigmoid(write_strength_logit.astype(jnp.float32)).reshape(
        local_heads, blocks, BLOCK
    )
    decay_logarithm = (
        -jnp.exp(head_decay_logarithm)[:, None]
        * jax.nn.softplus(decay_preactivation.astype(jnp.float32))
        + extra_log_decay
    )
    decay_logarithm = decay_logarithm.reshape(local_heads, blocks, BLOCK)
    decayed_queries, decayed_keys, updated_values, delta_corrections, scores, block_retention = (
        block_terms(query_block, key_block, value_block, decay_logarithm, strength)
    )
    fresh_wide = jnp.concatenate(
        [updated_values, jnp.zeros(updated_values.shape[:-1] + (DK,), jnp.float32)], axis=-1
    )
    inputs = tuple(
        (
            jnp.moveaxis(term, 1, 0)
            for term in (
                decayed_queries,
                decayed_keys,
                fresh_wide,
                delta_corrections,
                scores,
                block_retention,
            )
        )
    )
    identity_map = jnp.broadcast_to(jnp.eye(DK, dtype=jnp.float32), (local_heads, DK, DK))
    start_memory = jnp.concatenate(
        [jnp.zeros((local_heads, DK, DV), jnp.float32), identity_map], axis=-1
    )
    end_memory, outputs = lax.scan(carry_step, start_memory, inputs)
    local_output = outputs[..., :DV]
    projection_matrix = outputs[..., DV:]
    carried_end = end_memory[..., :DV]
    transfer = end_memory[..., DV:]
    _, incoming_rows = prefix(
        (transfer, carried_end), "ep", compose, (identity_map, jnp.zeros_like(carried_end))
    )
    attention_result = local_output + jnp.einsum(
        "xtyg,tgd->xtyd", projection_matrix, incoming_rows, precision=precise_setting
    )
    attn_rows = (
        attention_result.transpose(0, 2, 1, 3)
        .reshape(length, local_heads * DV)
        .astype(jnp.bfloat16)
    )
    summed = lax.psum_scatter(
        jnp.dot(attn_rows, output_weight, preferred_element_type=jnp.float32).astype(jnp.bfloat16),
        "tp",
        scatter_dimension=0,
        tiled=True,
    )
    widened = second_batch_tokens.astype(jnp.float32)
    normed = (
        widened
        * lax.rsqrt(jnp.mean(widened * widened, axis=-1, keepdims=True) + norm_eps)
        * expert_norm_scale
    ).astype(jnp.bfloat16)
    own_tokens = second_batch_tokens.shape[0]
    ep_count = lax.axis_size("ep")
    local_experts = EXPERTS // ep_count
    flat_ids = expert_choice_index.reshape(-1)
    one_hot = (flat_ids[:, None] == jnp.arange(EXPERTS, dtype=jnp.int32)[None, :]).astype(jnp.int32)
    slot_rank = jnp.sum((jnp.cumsum(one_hot, axis=0) - one_hot) * one_hot, axis=1)
    slot_index = flat_ids * CAP + slot_rank
    copy_token = jnp.arange(flat_ids.shape[0], dtype=jnp.int32) // TOPK
    slot_token = jnp.full((EXPERTS * CAP,), own_tokens, jnp.int32).at[slot_index].set(copy_token)
    outgoing = jnp.take(normed, slot_token, axis=0, mode="fill", fill_value=0).reshape(
        ep_count, local_experts, CAP, width_model
    )
    arrived = lax.all_to_all(outgoing, "ep", split_axis=0, concat_axis=0, tiled=True)
    gate_piece = lax.all_gather(expert_gate_weight, "tp", axis=1, tiled=True)
    up_piece = lax.all_gather(expert_up_weight, "tp", axis=1, tiled=True)
    down_piece = lax.all_gather(expert_down_weight, "tp", axis=1, tiled=True)
    gating = jnp.einsum("secd,efd->secf", arrived, gate_piece, preferred_element_type=jnp.float32)
    upward = jnp.einsum("secd,efd->secf", arrived, up_piece, preferred_element_type=jnp.float32)
    hidden = (jax.nn.silu(gating) * upward).astype(jnp.bfloat16)
    produced = jnp.einsum("secf,efd->secd", hidden, down_piece, preferred_element_type=jnp.float32)
    returned = lax.all_to_all(
        produced.astype(jnp.bfloat16), "ep", split_axis=0, concat_axis=0, tiled=True
    )
    flat_results = returned.reshape(EXPERTS * CAP, width_model)
    picked = (
        jnp.take(flat_results, slot_index, axis=0)
        .reshape(own_tokens, TOPK, width_model)
        .astype(jnp.float32)
    )
    leading = jax.nn.sigmoid(expert_logit_difference)
    mixing = group_router_weight[:, None] * jnp.stack([leading, 1.0 - leading], axis=-1)
    expert_out = jnp.sum(mixing[..., None] * picked, axis=1).astype(jnp.bfloat16)
    return (summed, expert_out)


def solution(mesh):
    in_specs = (
        P("ep", "tp"),
        P("ep", "tp"),
        P("ep", "tp"),
        P("tp", "ep"),
        P("tp", "ep"),
        P("tp"),
        P("tp", "ep"),
        P("tp", None),
        P(("ep", "tp"), None),
        P(),
        P(("ep", "tp"), None),
        P(("ep", "tp")),
        P(("ep", "tp")),
        P("ep", "tp", None),
        P("ep", "tp", None),
        P("ep", "tp", None),
    )
    out_specs = (P(("ep", "tp"), None), P(("ep", "tp"), None))
    return jax.shard_map(shards, mesh=mesh, in_specs=in_specs, out_specs=out_specs, check_vma=False)
```

profile of v0, /device:TPU:0, one launch (start us, length us, event | category | flops | bytes accessed | tf_op | source)
XLA Modules:
  0.0 520.2 jit_solution(1640668718798541853)
XLA Ops:
  11.6 1.4 scatter_custom_fusion
  13.5 3.3 gather_fusion
  16.9 3.1 broadcast_select_fusion
  20.0 5.6 %all-to-all-start = ((bf16[4,4,32,2048]{3,2,1,0:T(8,128)(2,1)}), bf16[4,4,32,2048]{3,2,1,0:T(8,128)(2,1)S(1)}, u32[]{:S(2)}, u32[]{:S(2)}) async-start(bf16[4,4,32,2048]{3,2,1,0:T(8,128)(2,1)} %broadcast_select_fusion), calls=%async_computation.1 | async-start | bytes 4194304 | tf_op jit(solution)/shard_map/all_to_all | solution.py:202
  29.5 3.0 fusion.52
  32.4 80.0 %custom-call.4 = f32[2,8,1,64,64]{3,4,2,1,0:T(8,128)} custom-call(f32[2,8,1,64,64]{4,3,2,1,0:T(8,128)} %fusion.52), custom_call_target="InvertDiagBlocksLowerTriangular" | custom-call | tf_op jit(solution)/shard_map/jit(_solve_triangular)/vmap(vmap())/triangular_solve | solution.py:52
  114.4 2.0 copy.100
  119.9 2.5 multiply_multiply_fusion
  125.6 2.0 fusion.50
  128.6 48.9 %while.26 = (s32[]{:T(128)}, f32[2,128,256]{2,1,0:T(8,128)S(1)}, f32[8,2,64,256]{3,2,0,1:T(8,128)}, f32[8,2]{1,0:T(8,128)}, f32[8,2,64,128]{3,2,0,1:T(8,128)}, /...) while((s32[]{:T(128)}, f32[2,128,256]{2,1,0:T(8,128)S(1)}, ...), condition=%wide.region_4.5_spmd, body=%wide.region_3.4_spmd.sunk | while | flops 176357376 | bytes 2231425 | solution.py:162
  128.6 1.2 convolution_subtract_fusion.2
  131.0 1.8 fusion.127
  133.5 1.3 convolution_add_fusion.4
  137.1 1.8 fusion.127
  139.6 1.3 convolution_add_fusion.4
  143.2 1.8 fusion.127
  145.7 1.3 convolution_add_fusion.4
  149.3 1.8 fusion.127
  151.8 1.3 convolution_add_fusion.4
  155.4 1.8 fusion.127
  157.9 1.3 convolution_add_fusion.4
  161.5 1.8 fusion.127
  164.0 1.3 convolution_add_fusion.4
  165.2 1.2 convolution_subtract_fusion.2
  167.6 1.8 fusion.127
  170.1 1.3 convolution_add_fusion.4
  171.4 1.3 convolution_subtract_fusion.2
  173.8 1.8 fusion.127
  176.3 1.3 convolution_add_fusion.4
  177.6 11.2 %all-gather = f32[8,128,128]{2,1,0:T(8,128)} all-gather(f32[2,128,128]{2,1,0:T(8,128)S(1)} %get-tuple-element.243), channel_id=2, replica_groups=mesh['ep'=4,'tp'=8] {'ep'}, dimensions={0}, use_global_device_ids=true | all-gather | bytes 655360 | tf_op jit(solution)/shard_map/all_gather | solution.py:18
  188.8 11.2 %all-gather.1 = f32[8,128,128]{2,1,0:T(8,128)} all-gather(f32[2,128,128]{2,1,0:T(8,128)S(1)} %get-tuple-element.242), channel_id=3, replica_groups=mesh['ep'=4,'tp'=8] {'ep'}, dimensions={0}, use_global_device_ids=true | all-gather | bytes 655360 | tf_op jit(solution)/shard_map/all_gather | solution.py:18
  200.1 4.0 while.27
  200.1 1.2 fusion.130
  201.4 1.2 fusion.130
  202.7 1.2 fusion.130
  204.1 1.8 fusion.55
  206.2 2.1 convolution_convert_fusion
  208.4 12.9 %fusion.26 = f32[4,4,32,1024]{3,2,1,0:T(8,128)} fusion(bf16[4,1024,2048]{2,1,0:T(8,128)(2,1)} %all-gather.8.cloned.1.call-done, bf16[4,4,32,2048]{3,2,1,0:T(8,128)(2,1)S(1)} %all-to-all-done), kind=kOutput, calls=%fused_computation.34 | convolution fusion | flops 2147483648 | bytes 20971520 | tf_op jit(solution)/shard_map/secd,efd->secf/dot_general | solution.py:207
  221.3 93.1 %all-gather.6.cloned.1.call-done = bf16[4,1024,2048]{2,1,0:T(8,128)(2,1)} async-done(((bf16[4,128,2048]{2,1,0:T(8,128)(2,1)}), bf16[4,1024,2048]{2,1,0:T(8,128)(2,1)}) %all-gather.6.cloned.1.call-update) | async-done | bytes 16777232 | tf_op jit(solution)/shard_map/all_gather | solution.py:203
  314.3 13.1 %fusion.36 = bf16[4,4,32,1024]{3,2,0,1:T(8,128)(2,1)} fusion(f32[4,4,32,1024]{3,2,1,0:T(8,128)} %fusion.26, bf16[4,1024,2048]{2,1,0:T(8,128)(2,1)} %all-gather.6.cloned.1.call-done, bf16[4,4,32,2048]{3,2,1,0:T(8,128)(2,1)S(1)} %all-to-all-done), kind=kOutput, calls=%fused_computation.42 | convolution fusion | flops 2150629376 | bytes 22020096 | tf_op jit(solution)/shard_map/secd,efd->secf/dot_general | solution.py:206
  327.4 137.8 %all-gather.10.cloned.1.call-done = bf16[4,1024,2048]{2,1,0:T(8,128)(2,1)} async-done(((bf16[4,128,2048]{2,1,0:T(8,128)(2,1)}), bf16[4,1024,2048]{2,1,0:T(8,128)(2,1)}) %all-gather.10.cloned.1.call-update) | async-done | bytes 16777232 | tf_op jit(solution)/shard_map/all_gather | solution.py:205
  465.3 8.5 %fusion.33 = bf16[4,4,32,2048]{3,2,0,1:T(8,128)(2,1)S(1)} fusion(bf16[4,4,32,1024]{3,2,0,1:T(8,128)(2,1)} %fusion.36, bf16[4,1024,2048]{2,1,0:T(8,128)(2,1)} %all-gather.10.cloned.1.call-done), kind=kOutput, calls=%fused_computation.40 | convolution fusion | flops 2148532224 | bytes 19922944 | tf_op jit(solution)/shard_map/secf,efd->secd/dot_general | solution.py:209
  473.7 1.6 copy.119
  475.3 4.0 all-to-all-start.1
  479.9 24.7 %all-to-all-done.1 = bf16[4,4,32,2048]{3,2,1,0:T(8,128)(2,1)S(1)} async-done(((bf16[4,4,32,2048]{3,2,1,0:T(8,128)(2,1)}), bf16[4,4,32,2048]{3,2,1,0:T(8,128)(2,1)S(1)}, u32[]{:S(2)}, u32[]{:S(2)}) %all-to-all-start.1) | async-done | bytes 2097184 | tf_op jit(solution)/shard_map/all_to_all | solution.py:210
  504.6 2.3 gather_fusion.1
  507.0 1.7 gather.15
  508.7 4.9 multiply_reduce_fusion
  (148 shorter events, 39.8 us)
Async XLA Ops:
  7.2 199.1 %copy-start = (bf16[256,2048]{1,0:T(8,128)(2,1)S(1)}, bf16[256,2048]{1,0:T(8,128)(2,1)}, u32[]{:S(2)}) copy-start(bf16[256,2048]{1,0:T(8,128)(2,1)} %param.27) | copy-start | bytes 3145732
  7.2 201.2 %all-gather.8.cloned.1.call-start = ((), (), s32[]{:S(2)}) async-start(), calls=%async_computation.5 | async-start | bytes 18874368 | tf_op jit(solution)/shard_map/all_gather | solution.py:204
  7.9 1.5 copy-start.11
  7.9 5.2 %copy-start.2 = (bf16[128,2048]{1,0:T(8,128)(2,1)S(1)}, bf16[128,2048]{1,0:T(8,128)(2,1)}, u32[]{:S(2)}) copy-start(bf16[128,2048]{1,0:T(8,128)(2,1)} %param.28) | copy-start | bytes 1572868
  7.9 5.4 %copy-start.14 = (f32[2048]{0:T(1024)S(1)}, f32[2048]{0:T(1024)}, u32[]{:S(2)}) copy-start(f32[2048]{0:T(1024)} %param.29) | copy-start | bytes 24580
  7.9 306.4 %all-gather.6.cloned.1.call-start = ((), (), s32[]{:S(2)}) async-start(), calls=%async_computation.4 | async-start | bytes 18874368 | tf_op jit(solution)/shard_map/all_gather | solution.py:203
  8.7 456.6 %all-gather.10.cloned.1.call-start = ((), (), s32[]{:S(2)}) async-start(), calls=%async_computation.6 | async-start | bytes 18874368 | tf_op jit(solution)/shard_map/all_gather | solution.py:205
  11.0 0.6 copy-start.9
  11.6 1.5 copy-start.17
  20.0 5.6 %copy-start.23 = (f32[2]{0:T(128)S(1)}, f32[2]{0:T(128)}, u32[]{:S(2)}) copy-start(f32[2]{0:T(128)} %param.25) | copy-start | bytes 28
  20.0 5.6 %copy-start.19 = (f32[2,512]{1,0:T(2,128)S(1)}, f32[2,512]{1,0:T(2,128)}, u32[]{:S(2)}) copy-start(f32[2,512]{1,0:T(2,128)} %param.26) | copy-start | bytes 12292
  20.0 5.6 %copy-start.20 = (bf16[2,512]{1,0:T(2,128)(2,1)S(1)}, bf16[2,512]{1,0:T(2,128)(2,1)}, u32[]{:S(2)}) copy-start(bf16[2,512]{1,0:T(2,128)(2,1)} %param.24) | copy-start | bytes 6148
  20.0 5.8 %copy-start.6 = (bf16[512,256]{1,0:T(8,128)(2,1)S(1)}, bf16[512,256]{1,0:T(8,128)(2,1)}, u32[]{:S(2)}) copy-start(bf16[512,256]{1,0:T(8,128)(2,1)} %param.21) | copy-start | bytes 786436
  20.0 188.4 %all-to-all-start = ((bf16[4,4,32,2048]{3,2,1,0:T(8,128)(2,1)}), bf16[4,4,32,2048]{3,2,1,0:T(8,128)(2,1)S(1)}, u32[]{:S(2)}, u32[]{:S(2)}) async-start(bf16[4,4,32,2048]{3,2,1,0:T(8,128)(2,1)} %broadcast_select_fusion), calls=%async_computation.1 | async-start | bytes 4194304 | tf_op jit(solution)/shard_map/all_to_all | solution.py:202
  25.6 488.0 %reduce-scatter.2.cloned.1.call-start = ((), (), s32[]{:S(2)}) async-start(), calls=%async_computation.3 | async-start | bytes 2359296 | tf_op jit(solution)/shard_map/reduce_scatter | solution.py:178
  28.6 0.6 copy-start.15
  28.7 0.8 copy-start.4
  116.8 0.6 copy-start.13
  118.1 4.3 copy-start.7
  122.4 2.0 copy-start.3
  122.4 3.1 copy-start.5
  122.4 3.1 copy-start.8
  122.4 3.1 copy-start.16
  123.6 4.0 copy-start.21
  475.3 4.0 copy-start.10
  475.3 4.2 copy-start.12
  475.3 4.4 copy-start.24
  475.3 4.4 copy-start.22
  475.3 4.6 copy-start.18
  475.3 29.3 %all-to-all-start.1 = ((bf16[4,4,32,2048]{3,2,1,0:T(8,128)(2,1)}), bf16[4,4,32,2048]{3,2,1,0:T(8,128)(2,1)S(1)}, u32[]{:S(2)}, u32[]{:S(2)}) async-start(bf16[4,4,32,2048]{3,2,1,0:T(8,128)(2,1)} %copy.119), calls=%async_computation.2 | async-start | bytes 4194304 | tf_op jit(solution)/shard_map/all_to_all | solution.py:210
  504.6 9.0 %copy-start.1 = (bf16[256,2048]{1,0:T(8,128)(2,1)S(1)}, bf16[256,2048]{1,0:T(8,128)(2,1)}, u32[]{:S(2)}) copy-start(bf16[256,2048]{1,0:T(8,128)(2,1)} %param.27) | copy-start | bytes 3145732
Sparse Core Ops, SparseCore 0:
  9.6 153.7 all-gather.7
  165.0 149.2 all-gather.5
  316.0 149.2 all-gather.9
  468.0 34.1 reduce-scatter.1
where the time goes:
time: 522 us; the launch traced here: 520 us
  waiting for transfers between devices  258 us (49%)
  other arithmetic  98.3 us (19%)
  matrix products  91.2 us (17%)
  local copies, waits for them, and re-layouts  26 us (5%)
  blocking collectives  22.5 us (4%)
  between operations  14.2 us (3%)
  starting transfers between devices  9.7 us (2%)
    all_gather x1, waiting for transfers between devices, shards(): down_piece = lax.all_gather(expert_down_weight, 'tp', axis=1, tiled=True)  138 us
    all_gather x1, waiting for transfers between devices, shards(): gate_piece = lax.all_gather(expert_gate_weight, 'tp', axis=1, tiled=True)  93.1 us
    another operation x2, other arithmetic, block_terms(): jax.scipy.linalg.solve_triangular(system, rhs_cols, lower=True, unit_diag...  80 us
    all_to_all x1, waiting for transfers between devices, shards(): lax.all_to_all(produced.astype(jnp.bfloat16), 'ep', split_axis=0, concat_...  24.7 us
    all_gather x2, blocking collectives, prefix(): pieces = jax.tree.map(lambda part: lax.all_gather(part, axis), value)  22.5 us
    dot_general x8, matrix products, carry_step(): jnp.einsum('hcj,hjv->hcv', scores, value_updates, precision=precise_setting)  14.2 us
    dot_general x1, matrix products, shards(): jnp.einsum('secd,efd->secf', arrived, gate_piece, preferred_element_type=...  13.1 us
    dot_general x1, matrix products, shards(): jnp.einsum('secd,efd->secf', arrived, up_piece, preferred_element_type=jn...  12.9 us
  transfers between devices with their start and end apart: 6, of which 3 were waited for; matrix products, arithmetic and copies ran while one was open for 41% of the time, Pallas kernels for 0%

commit v1 on v0

--- a/solution.py
+++ b/solution.py
@@ -11,6 +11,22 @@
 TOPK = 2
 precise_setting = lax.Precision.HIGHEST
 norm_eps = 1e-06
+
+
+def measure_page_for(view, mesh_ax, chunk):
+    z1, carry, state_next = (lax.psum(1, axis_name=mesh_ax), lax.axis_index(mesh_ax), view.shape[1])
+    series = [(num, (num + 1) % z1) for num in range(z1)]
+    res, even = (view, None)
+    for k0 in tuple(range(z1)):
+        v_next = (carry - k0) % z1
+        row_out = lax.ppermute(res, axis_name=mesh_ax, perm=series) if k0 < z1 - 1 else None
+        r_now = chunk(res, v_next * state_next)
+        main = r_now.shape[3]
+        if even is None:
+            even = jnp.zeros((*r_now.shape[:3], z1 * main, *r_now.shape[4:]), r_now.dtype)
+        even = lax.dynamic_update_slice_in_dim(even, r_now, v_next * main, axis=3)
+        res = row_out
+    return even
 
 
 def prefix(value, axis, join, neutral):
@@ -200,10 +216,15 @@
         ep_count, local_experts, CAP, width_model
     )
     arrived = lax.all_to_all(outgoing, "ep", split_axis=0, concat_axis=0, tiled=True)
-    gate_piece = lax.all_gather(expert_gate_weight, "tp", axis=1, tiled=True)
     up_piece = lax.all_gather(expert_up_weight, "tp", axis=1, tiled=True)
     down_piece = lax.all_gather(expert_down_weight, "tp", axis=1, tiled=True)
-    gating = jnp.einsum("secd,efd->secf", arrived, gate_piece, preferred_element_type=jnp.float32)
+    gating = measure_page_for(
+        expert_gate_weight,
+        "tp",
+        lambda shard, start: jnp.einsum(
+            "secd,efd->secf", arrived, shard, preferred_element_type=jnp.float32
+        ),
+    )
     upward = jnp.einsum("secd,efd->secf", arrived, up_piece, preferred_element_type=jnp.float32)
     hidden = (jax.nn.silu(gating) * upward).astype(jnp.bfloat16)
     produced = jnp.einsum("secf,efd->secd", hidden, down_piece, preferred_element_type=jnp.float32)

time: 522 us -> 580 us (1.11)
  the two profiles are of different devices: /device:TPU:0 before, /device:TPU:8 now
where the time goes in v1:
time: 580 us; the launch traced here: 578 us
  waiting for transfers between devices  185 us (32%)
  starting transfers between devices  164 us (28%)
  other arithmetic  92.6 us (16%)
  matrix products  86.4 us (15%)
  blocking collectives  21.7 us (4%)
  between operations  14.5 us (2%)
  local copies, waits for them, and re-layouts  13.4 us (2%)
    ppermute x7, waiting for transfers between devices, measure_page_for(): lax.ppermute(res, axis_name=mesh_ax, perm=series)  160 us
    ppermute x7, starting transfers between devices, measure_page_for(): lax.ppermute(res, axis_name=mesh_ax, perm=series)  155 us
    another operation x2, other arithmetic, block_terms(): jax.scipy.linalg.solve_triangular(system, rhs_cols, lower=True, unit_diag...  78.6 us
    all_to_all x1, waiting for transfers between devices, shards(): lax.all_to_all(produced.astype(jnp.bfloat16), 'ep', split_axis=0, concat_...  24.3 us
    dot_general x8, matrix products, shards(): jnp.einsum('secd,efd->secf', arrived, shard, preferred_element_type=jnp.f...  23 us
    all_gather x2, blocking collectives, prefix(): pieces = jax.tree.map(lambda part: lax.all_gather(part, axis), value)  21.7 us
    dot_general x8, matrix products, carry_step(): jnp.einsum('hcj,hjv->hcv', scores, value_updates, precision=precise_setting)  14.1 us
    dot_general x1, matrix products, shards(): jnp.einsum('secd,efd->secf', arrived, up_piece, preferred_element_type=jn...  12.2 us
  transfers between devices with their start and end apart: 12, of which 6 were waited for; matrix products, arithmetic and copies ran while one was open for 33% of the time, Pallas kernels for 0%

profile of v1, /device:TPU:8, one launch (start us, length us, event | category | flops | bytes accessed | tf_op | source)
XLA Modules:
  0.0 578.3 jit_solution(4147608489789610130)
XLA Ops:
  8.8 51.0 %collective-permute-done = bf16[4,128,2048]{2,1,0:T(8,128)(2,1)} collective-permute-done((bf16[4,128,2048]{2,1,0:T(8,128)(2,1)}, bf16[4,128,2048]{2,1,0:T(8,128)(2,1)}, u32[]{:S(2)}, u32[]{:S(2)}) %collective-permute-start) | collective-permute-done | bytes 2097184 | tf_op jit(solution)/shard_map/ppermute | solution.py:22
  59.8 20.9 %collective-permute-start.1 = (bf16[4,128,2048]{2,1,0:T(8,128)(2,1)}, bf16[4,128,2048]{2,1,0:T(8,128)(2,1)}, u32[]{:S(2)}, u32[]{:S(2)}) collective-permute-start(bf16[4,128,2048]{2,1,0:T(8,128)(2,1)} %collective-permute-done), channel_id=1, source_target_pairs={{0,1},{1,2},{2,3},{3,4},{4,5},{5,6},{6,7},{7,0},{8,9},{9,10},{10,1... | collective-permute-start | bytes 6291464 | tf_op jit(solution)/shard_map/ppermute | solution.py:22
  82.3 1.4 scatter_custom_fusion
  83.7 46.9 %collective-permute-done.1 = bf16[4,128,2048]{2,1,0:T(8,128)(2,1)} collective-permute-done((bf16[4,128,2048]{2,1,0:T(8,128)(2,1)}, bf16[4,128,2048]{2,1,0:T(8,128)(2,1)}, u32[]{:S(2)}, u32[]{:S(2)}) %collective-permute-start.1) | collective-permute-done | bytes 2097184 | tf_op jit(solution)/shard_map/ppermute | solution.py:22
  130.6 49.2 %collective-permute-start.2 = (bf16[4,128,2048]{2,1,0:T(8,128)(2,1)}, bf16[4,128,2048]{2,1,0:T(8,128)(2,1)}, u32[]{:S(2)}, u32[]{:S(2)}) collective-permute-start(bf16[4,128,2048]{2,1,0:T(8,128)(2,1)} %collective-permute-done.1), channel_id=1, source_target_pairs={{0,1},{1,2},{2,3},{3,4},{4,5},{5,6},{6,7},{7,0},{8,9},{9,10},{10,1... | collective-permute-start | bytes 6291464 | tf_op jit(solution)/shard_map/ppermute | solution.py:22
  180.3 3.3 gather_fusion
  183.7 3.1 broadcast_select_fusion
  186.8 4.6 all-to-all-start
  191.8 9.6 %collective-permute-done.2 = bf16[4,128,2048]{2,1,0:T(8,128)(2,1)} collective-permute-done((bf16[4,128,2048]{2,1,0:T(8,128)(2,1)}, bf16[4,128,2048]{2,1,0:T(8,128)(2,1)}, u32[]{:S(2)}, u32[]{:S(2)}) %collective-permute-start.2) | collective-permute-done | bytes 2097184 | tf_op jit(solution)/shard_map/ppermute | solution.py:22
  201.5 15.4 %collective-permute-start.3 = (bf16[4,128,2048]{2,1,0:T(8,128)(2,1)}, bf16[4,128,2048]{2,1,0:T(8,128)(2,1)}, u32[]{:S(2)}, u32[]{:S(2)}) collective-permute-start(bf16[4,128,2048]{2,1,0:T(8,128)(2,1)} %collective-permute-done.2), channel_id=1, source_target_pairs={{0,1},{1,2},{2,3},{3,4},{4,5},{5,6},{6,7},{7,0},{8,9},{9,10},{10,1... | collective-permute-start | bytes 6291464 | tf_op jit(solution)/shard_map/ppermute | solution.py:22
  218.0 1.3 fusion.59
  219.4 24.5 %collective-permute-done.3 = bf16[4,128,2048]{2,1,0:T(8,128)(2,1)} collective-permute-done((bf16[4,128,2048]{2,1,0:T(8,128)(2,1)}, bf16[4,128,2048]{2,1,0:T(8,128)(2,1)}, u32[]{:S(2)}, u32[]{:S(2)}) %collective-permute-start.3) | collective-permute-done | bytes 2097184 | tf_op jit(solution)/shard_map/ppermute | solution.py:22
  243.9 35.0 %collective-permute-start.4 = (bf16[4,128,2048]{2,1,0:T(8,128)(2,1)}, bf16[4,128,2048]{2,1,0:T(8,128)(2,1)}, u32[]{:S(2)}, u32[]{:S(2)}) collective-permute-start(bf16[4,128,2048]{2,1,0:T(8,128)(2,1)} %collective-permute-done.3), channel_id=1, source_target_pairs={{0,1},{1,2},{2,3},{3,4},{4,5},{5,6},{6,7},{7,0},{8,9},{9,10},{10,1... | collective-permute-start | bytes 6291464 | tf_op jit(solution)/shard_map/ppermute | solution.py:22
  279.0 78.6 %custom-call.4 = f32[2,8,1,64,64]{3,4,2,1,0:T(8,128)S(1)} custom-call(f32[2,8,1,64,64]{4,3,2,1,0:T(8,128)S(1)} %fusion.59), custom_call_target="InvertDiagBlocksLowerTriangular" | custom-call | tf_op jit(solution)/shard_map/jit(_solve_triangular)/vmap(vmap())/triangular_solve | solution.py:68
  359.1 1.4 multiply_multiply_fusion
  362.8 2.0 fusion.57
  364.8 34.8 %collective-permute-start.5 = (bf16[4,128,2048]{2,1,0:T(8,128)(2,1)}, bf16[4,128,2048]{2,1,0:T(8,128)(2,1)}, u32[]{:S(2)}, u32[]{:S(2)}) collective-permute-start(bf16[4,128,2048]{2,1,0:T(8,128)(2,1)} %collective-permute-done.4), channel_id=1, source_target_pairs={{0,1},{1,2},{2,3},{3,4},{4,5},{5,6},{6,7},{7,0},{8,9},{9,10},{10,1... | collective-permute-start | bytes 6291464 | tf_op jit(solution)/shard_map/ppermute | solution.py:22
  399.6 35.7 %while.26 = (s32[]{:T(128)}, f32[2,128,256]{2,1,0:T(8,128)S(1)}, f32[8,2,64,256]{3,2,0,1:T(8,128)}, f32[8,2]{1,0:T(8,128)S(1)}, f32[8,2,64,128]{3,2,0,1:T(8,128)...) while((s32[]{:T(128)}, f32[2,128,256]{2,1,0:T(8,128)S(1)}, ...), condition=%wide.region_4.5_spmd, body=%wide.region_3.4_spmd.sunk | while | flops 176357376 | bytes 2231425 | solution.py:178
  401.0 1.7 fusion.191
  402.8 1.3 convolution_add_fusion.4
  405.5 1.8 fusion.191
  409.9 1.8 fusion.191
  411.7 1.3 convolution_add_fusion.4
  414.4 1.8 fusion.191
  418.9 1.8 fusion.191
  423.4 1.7 fusion.191
  427.8 1.8 fusion.191
  432.3 1.8 fusion.191
  435.3 10.9 %all-gather = f32[8,128,128]{2,1,0:T(8,128)S(1)} all-gather(f32[2,128,128]{2,1,0:T(8,128)S(1)} %get-tuple-element.243), channel_id=2, replica_groups=mesh['ep'=4,'tp'=8] {'ep'}, dimensions={0}, use_global_device_ids=true | all-gather | bytes 655360 | tf_op jit(solution)/shard_map/all_gather | solution.py:34
  446.2 10.8 %all-gather.1 = f32[8,128,128]{2,1,0:T(8,128)S(1)} all-gather(f32[2,128,128]{2,1,0:T(8,128)S(1)} %get-tuple-element.242), channel_id=3, replica_groups=mesh['ep'=4,'tp'=8] {'ep'}, dimensions={0}, use_global_device_ids=true | all-gather | bytes 655360 | tf_op jit(solution)/shard_map/all_gather | solution.py:34
  458.9 2.1 convolution_convert_fusion
  461.4 2.9 fusion.66
  464.4 2.9 fusion.72
  467.3 3.0 fusion.78
  470.3 3.0 fusion.84
  473.3 3.0 fusion.90
  476.2 3.0 fusion.96
  479.2 3.0 fusion.102
  482.2 27.5 %collective-permute-done.6 = bf16[4,128,2048]{2,1,0:T(8,128)(2,1)S(1)} collective-permute-done((bf16[4,128,2048]{2,1,0:T(8,128)(2,1)}, bf16[4,128,2048]{2,1,0:T(8,128)(2,1)S(1)}, u32[]{:S(2)}, u32[]{:S(2)}) %collective-permute-start.6) | collective-permute-done | bytes 2097184 | tf_op jit(solution)/shard_map/ppermute | solution.py:22
  509.7 2.3 fusion.108
  512.0 12.2 %fusion.50 = bf16[4,4,32,1024]{3,2,0,1:T(8,128)(2,1)S(1)} fusion(f32[4,4,32,1024]{3,2,0,1:T(8,128)S(1)} %fusion.108, bf16[4,1024,2048]{2,1,0:T(8,128)(2,1)} %all-gather.5.cloned.1.call-done, bf16[4,4,32,2048]{3,2,1,0:T(8,128)(2,1)} %all-to-all-done), kind=kOutput, calls=%fused_computation.56 | convolution fusion | flops 2150629376 | bytes 22020096 | tf_op jit(solution)/shard_map/secd,efd->secf/dot_general | solution.py:228
  524.2 8.1 %fusion.31 = bf16[4,4,32,2048]{3,2,0,1:T(8,128)(2,1)S(1)} fusion(bf16[4,4,32,1024]{3,2,0,1:T(8,128)(2,1)S(1)} %fusion.50, bf16[4,1024,2048]{2,1,0:T(8,128)(2,1)} %all-gather.7.cloned.1.call-done), kind=kOutput, calls=%fused_computation.38 | convolution fusion | flops 2148532224 | bytes 19922944 | tf_op jit(solution)/shard_map/secf,efd->secd/dot_general | solution.py:230
  532.4 1.6 copy.133
  534.0 4.0 all-to-all-start.1
  538.5 24.3 %all-to-all-done.1 = bf16[4,4,32,2048]{3,2,1,0:T(8,128)(2,1)S(1)} async-done(((bf16[4,4,32,2048]{3,2,1,0:T(8,128)(2,1)}), bf16[4,4,32,2048]{3,2,1,0:T(8,128)(2,1)S(1)}, u32[]{:S(2)}, u32[]{:S(2)}) %all-to-all-start.1) | async-done | bytes 2097184 | tf_op jit(solution)/shard_map/all_to_all | solution.py:231
  562.8 2.3 gather_fusion.1
  565.1 1.7 gather.15
  566.9 4.9 multiply_reduce_fusion
  (147 shorter events, 31.3 us)
Async XLA Ops:
  7.2 451.7 %copy-start = (bf16[256,2048]{1,0:T(8,128)(2,1)S(1)}, bf16[256,2048]{1,0:T(8,128)(2,1)}, u32[]{:S(2)}) copy-start(bf16[256,2048]{1,0:T(8,128)(2,1)} %param.27) | copy-start | bytes 3145732
  7.2 73.5 %copy-start.6 = (s32[128,2]{0,1:T(2,128)S(1)}, s32[128,2]{0,1:T(2,128)}, u32[]{:S(2)}) copy-start(s32[128,2]{0,1:T(2,128)} %param.30) | copy-start | bytes 3076
  7.2 172.7 %copy-start.2 = (bf16[128,2048]{1,0:T(8,128)(2,1)S(1)}, bf16[128,2048]{1,0:T(8,128)(2,1)}, u32[]{:S(2)}) copy-start(bf16[128,2048]{1,0:T(8,128)(2,1)} %param.28) | copy-start | bytes 1572868
  7.2 172.9 %copy-start.7 = (f32[2048]{0:T(1024)S(1)}, f32[2048]{0:T(1024)}, u32[]{:S(2)}) copy-start(f32[2048]{0:T(1024)} %param.29) | copy-start | bytes 24580
  7.2 504.8 %all-gather.5.cloned.1.call-start = ((), (), s32[]{:S(2)}) async-start(), calls=%async_computation.4 | async-start | bytes 18874368 | tf_op jit(solution)/shard_map/all_gather | solution.py:219
  7.9 516.3 %all-gather.7.cloned.1.call-start = ((), (), s32[]{:S(2)}) async-start(), calls=%async_computation.5 | async-start | bytes 18874368 | tf_op jit(solution)/shard_map/all_gather | solution.py:220
  8.7 51.1 %collective-permute-start = (bf16[4,128,2048]{2,1,0:T(8,128)(2,1)}, bf16[4,128,2048]{2,1,0:T(8,128)(2,1)}, u32[]{:S(2)}, u32[]{:S(2)}) collective-permute-start(bf16[4,128,2048]{2,1,0:T(8,128)(2,1)} %param.33), channel_id=1, source_target_pairs={{0,1},{1,2},{2,3},{3,4},{4,5},{5,6},{6,7},{7,0},{8,9},{9,10},{10,1... | collective-permute-start | bytes 6291464 | tf_op jit(solution)/shard_map/ppermute | solution.py:22
  59.8 70.8 %collective-permute-start.1 = (bf16[4,128,2048]{2,1,0:T(8,128)(2,1)}, bf16[4,128,2048]{2,1,0:T(8,128)(2,1)}, u32[]{:S(2)}, u32[]{:S(2)}) collective-permute-start(bf16[4,128,2048]{2,1,0:T(8,128)(2,1)} %collective-permute-done), channel_id=1, source_target_pairs={{0,1},{1,2},{2,3},{3,4},{4,5},{5,6},{6,7},{7,0},{8,9},{9,10},{10,1... | collective-permute-start | bytes 6291464 | tf_op jit(solution)/shard_map/ppermute | solution.py:22
  130.6 70.8 %collective-permute-start.2 = (bf16[4,128,2048]{2,1,0:T(8,128)(2,1)}, bf16[4,128,2048]{2,1,0:T(8,128)(2,1)}, u32[]{:S(2)}, u32[]{:S(2)}) collective-permute-start(bf16[4,128,2048]{2,1,0:T(8,128)(2,1)} %collective-permute-done.1), channel_id=1, source_target_pairs={{0,1},{1,2},{2,3},{3,4},{4,5},{5,6},{6,7},{7,0},{8,9},{9,10},{10,1... | collective-permute-start | bytes 6291464 | tf_op jit(solution)/shard_map/ppermute | solution.py:22
  186.8 4.7 copy-start.3
  186.8 4.9 copy-start.13
  186.8 4.9 copy-start.8
  186.8 5.0 copy-start.10
  186.8 30.2 %copy-start.9 = (bf16[2,512]{1,0:T(2,128)(2,1)S(1)}, bf16[2,512]{1,0:T(2,128)(2,1)}, u32[]{:S(2)}) copy-start(bf16[2,512]{1,0:T(2,128)(2,1)} %param.23) | copy-start | bytes 6148
  186.8 30.2 %copy-start.5 = (bf16[512,256]{1,0:T(8,128)(2,1)S(1)}, bf16[512,256]{1,0:T(8,128)(2,1)}, u32[]{:S(2)}) copy-start(bf16[512,256]{1,0:T(8,128)(2,1)} %param.20) | copy-start | bytes 786436
  186.8 274.3 %all-to-all-start = ((bf16[4,4,32,2048]{3,2,1,0:T(8,128)(2,1)}), bf16[4,4,32,2048]{3,2,1,0:T(8,128)(2,1)}, u32[]{:S(2)}, u32[]{:S(2)}) async-start(bf16[4,4,32,2048]{3,2,1,0:T(8,128)(2,1)} %broadcast_select_fusion), calls=%async_computation.1 | async-start | bytes 4194304 | tf_op jit(solution)/shard_map/all_to_all | solution.py:218
  191.4 380.3 %reduce-scatter.2.cloned.1.call-start = ((), (), s32[]{:S(2)}) async-start(), calls=%async_computation.3 | async-start | bytes 2359296 | tf_op jit(solution)/shard_map/reduce_scatter | solution.py:194
  201.5 42.5 %collective-permute-start.3 = (bf16[4,128,2048]{2,1,0:T(8,128)(2,1)}, bf16[4,128,2048]{2,1,0:T(8,128)(2,1)}, u32[]{:S(2)}, u32[]{:S(2)}) collective-permute-start(bf16[4,128,2048]{2,1,0:T(8,128)(2,1)} %collective-permute-done.2), channel_id=1, source_target_pairs={{0,1},{1,2},{2,3},{3,4},{4,5},{5,6},{6,7},{7,0},{8,9},{9,10},{10,1... | collective-permute-start | bytes 6291464 | tf_op jit(solution)/shard_map/ppermute | solution.py:22
  243.9 120.9 %collective-permute-start.4 = (bf16[4,128,2048]{2,1,0:T(8,128)(2,1)}, bf16[4,128,2048]{2,1,0:T(8,128)(2,1)}, u32[]{:S(2)}, u32[]{:S(2)}) collective-permute-start(bf16[4,128,2048]{2,1,0:T(8,128)(2,1)} %collective-permute-done.3), channel_id=1, source_target_pairs={{0,1},{1,2},{2,3},{3,4},{4,5},{5,6},{6,7},{7,0},{8,9},{9,10},{10,1... | collective-permute-start | bytes 6291464 | tf_op jit(solution)/shard_map/ppermute | solution.py:22
  361.6 3.2 copy-start.11
  364.8 99.5 %collective-permute-start.5 = (bf16[4,128,2048]{2,1,0:T(8,128)(2,1)}, bf16[4,128,2048]{2,1,0:T(8,128)(2,1)}, u32[]{:S(2)}, u32[]{:S(2)}) collective-permute-start(bf16[4,128,2048]{2,1,0:T(8,128)(2,1)} %collective-permute-done.4), channel_id=1, source_target_pairs={{0,1},{1,2},{2,3},{3,4},{4,5},{5,6},{6,7},{7,0},{8,9},{9,10},{10,1... | collective-permute-start | bytes 6291464 | tf_op jit(solution)/shard_map/ppermute | solution.py:22
  446.2 11.7 %copy-start.4 = (f32[8,2,64,256]{3,2,0,1:T(8,128)S(1)}, f32[8,2,64,256]{3,2,0,1:T(8,128)}, u32[]{:S(2)}) copy-start(f32[8,2,64,256]{3,2,0,1:T(8,128)} %get-tuple-element.144) | copy-start | bytes 3145732
  464.3 45.4 %collective-permute-start.6 = (bf16[4,128,2048]{2,1,0:T(8,128)(2,1)}, bf16[4,128,2048]{2,1,0:T(8,128)(2,1)S(1)}, u32[]{:S(2)}, u32[]{:S(2)}) collective-permute-start(bf16[4,128,2048]{2,1,0:T(8,128)(2,1)} %collective-permute-done.5), channel_id=1, source_target_pairs={{0,1},{1,2},{2,3},{3,4},{4,5},{5,6},{6,7},{7,0},{8,9},{9,10},{10,1... | collective-permute-start | bytes 6291464 | tf_op jit(solution)/shard_map/ppermute | solution.py:22
  534.0 4.3 copy-start.14
  534.0 4.4 copy-start.12
  534.0 28.8 %all-to-all-start.1 = ((bf16[4,4,32,2048]{3,2,1,0:T(8,128)(2,1)}), bf16[4,4,32,2048]{3,2,1,0:T(8,128)(2,1)S(1)}, u32[]{:S(2)}, u32[]{:S(2)}) async-start(bf16[4,4,32,2048]{3,2,1,0:T(8,128)(2,1)} %copy.133), calls=%async_computation.2 | async-start | bytes 4194304 | tf_op jit(solution)/shard_map/all_to_all | solution.py:231
  562.8 9.0 %copy-start.1 = (bf16[256,2048]{1,0:T(8,128)(2,1)S(1)}, bf16[256,2048]{1,0:T(8,128)(2,1)}, u32[]{:S(2)}) copy-start(bf16[256,2048]{1,0:T(8,128)(2,1)} %param.27) | copy-start | bytes 3145732
Sparse Core Ops, SparseCore 0:
  9.6 211.4 all-gather.4
  222.7 191.9 all-gather.6
  461.1 36.5 reduce-scatter.1
